TPU v7x, 32 devices: a whole 2x2x4 slice. The times are simulated.
32 devices in a mesh: sp: 16 (over z, y, core), tp: 2 (over x).
Axes of the slice: x: 2, y: 2, z: 4, core: 2. Of those that a mesh axis runs over, the one named last changes fastest.
Arguments:
- inputs: bfloat16 [2, 2048, 1024], P(None, 'sp'), may hold values from -6 to 6
- queries: bfloat16 [2, 2048, 4, 128], P(None, 'sp', 'tp'), may hold values from -6 to 6
- values: bfloat16 [2, 2048, 4, 256], P(None, 'sp', 'tp'), may hold values from -6 to 6
- out_grad: bfloat16 [2, 2048, 4, 256], P(None, 'sp', 'tp'), may hold values from -6 to 6
- key_weight: bfloat16 [1024, 4, 128], P(None, 'tp'), may hold values from -6 to 6
- decay_ahead: float32 [4], P('tp'), may hold values from -2.9 to 2.2
- decay_behind: float32 [4], P('tp'), may hold values from -2.9 to 2.2
Outputs:
- query_grad: bfloat16 [2, 2048, 4, 128], P(None, 'sp', 'tp')
- value_grad: bfloat16 [2, 2048, 4, 256], P(None, 'sp', 'tp')
- input_grad: bfloat16 [2, 2048, 1024], P('tp', 'sp')
- weight_grad: float32 [1024, 4, 128], P('sp', 'tp')
- decay_grad: float32 [2, 4], P(None, 'tp')
All inputs are finite; a program needn't handle non-finite values.
Results may differ from a plain program's by a relative error of at most 0.015.
Values may be sent and summed in bfloat16 or wider, within the bound.
A program may use at most 256 MiB of HBM per device.

v0:
```python
import math
import jax
import jax.numpy as jnp
from jax import lax
from jax.sharding import PartitionSpec as P

HIGHEST = lax.Precision.HIGHEST


def prefix(value, axis, join, neutral, backward):
    count, mine = (lax.axis_size(axis), lax.axis_index(axis))
    pieces = jax.tree.map(lambda part: lax.all_gather(part, axis), value)
    if backward:
        pieces = jax.tree.map(lambda part: part[::-1], pieces)
        mine = count - 1 - mine
    subtotal = jax.tree.map(
        lambda part, zero: jnp.full_like(part, 0) + jnp.asarray(zero, part.dtype), value, neutral
    )

    def step(position, subtotal):
        longer = join(subtotal, jax.tree.map(lambda part: part[position], pieces))
        return jax.tree.map(lambda new, old: jnp.where(position < mine, new, old), longer, subtotal)

    return lax.fori_loop(0, count - 1, step, subtotal)


def own_rows(contribution, rows, axis):
    whole = contribution(jnp.int32(0), rows * lax.axis_size(axis))
    return lax.psum_scatter(whole, axis, scatter_dimension=0, tiled=True)


def summed_rows(product, rows, axis):
    everything = product(jnp.int32(0), lax.axis_size(axis) * rows)
    own = lax.psum_scatter(everything.astype(jnp.bfloat16), axis, scatter_dimension=0, tiled=True)
    return own.astype(jnp.float32)


def link_states(earlier, later):
    return (
        earlier[0] * later[0],
        later[0] * earlier[1] + later[1],
        earlier[2] * later[2],
        later[2] * earlier[3] + later[3],
    )


def shards(inputs, queries, values, out_grad, key_weight, decay_ahead, decay_behind):
    batch_seqs, length, in_width = inputs.shape
    devices = lax.axis_size("sp")
    my_index = lax.axis_index("sp").astype(jnp.float32)
    all_tokens = length * devices
    key_scale = 1.0 / math.sqrt(in_width * queries.shape[3] * all_tokens)
    rate_ahead = jax.nn.log_sigmoid(decay_ahead) / all_tokens
    rate_behind = jax.nn.log_sigmoid(decay_behind) / all_tokens
    key_raw = jnp.einsum(
        "bld,dhk->blhk", inputs, key_weight, preferred_element_type=jnp.float32
    ).astype(jnp.bfloat16)
    keys = key_raw.astype(jnp.float32) * key_scale
    query_wide = queries.astype(jnp.float32)
    value_wide = values.astype(jnp.float32)
    grad_wide = out_grad.astype(jnp.float32)
    offsets = jnp.arange(length, dtype=jnp.float32)
    distance = offsets[:, None] - offsets[None, :]
    mask_ahead = jnp.where(
        distance[None] >= 0, jnp.exp(distance[None] * rate_ahead[:, None, None]), 0.0
    )
    mask_behind = jnp.where(
        distance[None] <= 0, jnp.exp(-distance[None] * rate_behind[:, None, None]), 0.0
    )
    mask_both = (mask_ahead + mask_behind)[None]
    keep_ahead = jnp.exp((length - 1.0 - offsets)[:, None] * rate_ahead[None])[None, :, :, None]
    keep_behind = jnp.exp(offsets[:, None] * rate_behind[None])[None, :, :, None]
    reach_ahead = jnp.exp((offsets + 1.0)[:, None] * rate_ahead[None])[None, :, :, None]
    reach_behind = jnp.exp((length - offsets)[:, None] * rate_behind[None])[None, :, :, None]
    scores = (
        jnp.einsum("bthk,bshk->bhts", queries, key_raw, preferred_element_type=jnp.float32)
        * key_scale
    )
    grad_scores = jnp.einsum(
        "bthv,bshv->bhts", out_grad, values, preferred_element_type=jnp.float32
    )
    sums_ahead = jnp.einsum("bshk,bshv->bhkv", keys * keep_ahead, value_wide, precision=HIGHEST)
    sums_behind = jnp.einsum("bshk,bshv->bhkv", keys * keep_behind, value_wide, precision=HIGHEST)
    pulls_ahead = jnp.einsum(
        "bthk,bthv->bhkv", query_wide * reach_ahead, grad_wide, precision=HIGHEST
    )
    pulls_behind = jnp.einsum(
        "bthk,bthv->bhkv", query_wide * reach_behind, grad_wide, precision=HIGHEST
    )
    span_ahead = jnp.exp(length * rate_ahead).reshape(1, -1, 1, 1)
    span_behind = jnp.exp(length * rate_behind).reshape(1, -1, 1, 1)
    unit_span = jnp.ones_like(span_ahead)
    zero_state = jnp.zeros_like(sums_ahead)
    upward = prefix(
        (span_ahead, sums_ahead, span_behind, pulls_behind),
        "sp",
        link_states,
        (unit_span, zero_state, unit_span, zero_state),
        False,
    )
    downward = prefix(
        (span_behind, sums_behind, span_ahead, pulls_ahead),
        "sp",
        link_states,
        (unit_span, zero_state, unit_span, zero_state),
        True,
    )
    state_ahead, pull_behind = (upward[1], upward[3])
    state_behind, pull_ahead = (downward[1], downward[3])
    out_ahead = jnp.einsum(
        "bhts,bshv->bthv", scores * mask_ahead[None], value_wide, precision=HIGHEST
    )
    out_ahead = out_ahead + jnp.einsum(
        "bthk,bhkv->bthv", query_wide * reach_ahead, state_ahead, precision=HIGHEST
    )
    out_behind = jnp.einsum(
        "bhts,bshv->bthv", scores * mask_behind[None], value_wide, precision=HIGHEST
    )
    out_behind = out_behind + jnp.einsum(
        "bthk,bhkv->bthv", query_wide * reach_behind, state_behind, precision=HIGHEST
    )
    grad_q = jnp.einsum("bhts,bshk->bthk", grad_scores * mask_both, keys, precision=HIGHEST)
    grad_q = grad_q + reach_ahead * jnp.einsum(
        "bthv,bhkv->bthk", grad_wide, state_ahead, precision=HIGHEST
    )
    grad_q = grad_q + reach_behind * jnp.einsum(
        "bthv,bhkv->bthk", grad_wide, state_behind, precision=HIGHEST
    )
    grad_k_ahead = jnp.einsum(
        "bhts,bthk->bshk", grad_scores * mask_ahead[None], query_wide, precision=HIGHEST
    )
    grad_k_ahead = grad_k_ahead + keep_ahead * jnp.einsum(
        "bshv,bhkv->bshk", value_wide, pull_ahead, precision=HIGHEST
    )
    grad_k_behind = jnp.einsum(
        "bhts,bthk->bshk", grad_scores * mask_behind[None], query_wide, precision=HIGHEST
    )
    grad_k_behind = grad_k_behind + keep_behind * jnp.einsum(
        "bshv,bhkv->bshk", value_wide, pull_behind, precision=HIGHEST
    )
    grad_v = jnp.einsum("bhts,bthv->bshv", scores * mask_both, grad_wide, precision=HIGHEST)
    grad_v = grad_v + keep_ahead * jnp.einsum(
        "bshk,bhkv->bshv", keys, pull_ahead, precision=HIGHEST
    )
    grad_v = grad_v + keep_behind * jnp.einsum(
        "bshk,bhkv->bshv", keys, pull_behind, precision=HIGHEST
    )
    positions = (my_index * length + offsets)[None, :, None]
    out_dot_ahead = jnp.sum(positions * jnp.sum(out_ahead * grad_wide, axis=3), axis=(0, 1))
    key_dot_ahead = jnp.sum(positions * jnp.sum(keys * grad_k_ahead, axis=3), axis=(0, 1))
    out_dot_behind = jnp.sum(positions * jnp.sum(out_behind * grad_wide, axis=3), axis=(0, 1))
    key_dot_behind = jnp.sum(positions * jnp.sum(keys * grad_k_behind, axis=3), axis=(0, 1))
    local_sums = jnp.stack([out_dot_ahead - key_dot_ahead, key_dot_behind - out_dot_behind])
    rate_sums = lax.psum(local_sums, "sp")
    slopes = jnp.stack([jax.nn.sigmoid(-decay_ahead), jax.nn.sigmoid(-decay_behind)]) / all_tokens
    decay_grad = rate_sums * slopes
    key_grad_raw = ((grad_k_ahead + grad_k_behind) * key_scale).astype(jnp.bfloat16)

    def weight_rows(start, row_count):
        piece = lax.dynamic_slice_in_dim(inputs, start, row_count, 2)
        return jnp.einsum("bld,blhk->dhk", piece, key_grad_raw, preferred_element_type=jnp.float32)

    weight_grad = own_rows(weight_rows, in_width // devices, "sp")

    def input_rows(start, row_count):
        piece = lax.dynamic_slice_in_dim(key_grad_raw, start, row_count, 0)
        return jnp.einsum("blhk,dhk->bld", piece, key_weight, preferred_element_type=jnp.float32)

    input_grad = summed_rows(input_rows, batch_seqs // lax.axis_size("tp"), "tp").astype(
        jnp.bfloat16
    )
    return (
        grad_q.astype(jnp.bfloat16),
        grad_v.astype(jnp.bfloat16),
        input_grad,
        weight_grad,
        decay_grad,
    )


def solution(mesh):
    in_specs = (
        P(None, "sp", None),
        P(None, "sp", "tp", None),
        P(None, "sp", "tp", None),
        P(None, "sp", "tp", None),
        P(None, "tp", None),
        P("tp"),
        P("tp"),
    )
    out_specs = (
        P(None, "sp", "tp", None),
        P(None, "sp", "tp", None),
        P("tp", "sp", None),
        P("sp", "tp", None),
        P(None, "tp"),
    )
    return jax.shard_map(shards, mesh=mesh, in_specs=in_specs, out_specs=out_specs, check_vma=False)
```

profile of v0, /device:TPU:0, one launch (start us, length us, event | category | flops | bytes accessed | tf_op | source)
XLA Modules:
  0.0 462.7 jit_solution(7390019577858132643)
XLA Ops:
  10.9 2.1 fusion.41
  14.8 2.1 fusion.37
  17.1 2.1 fusion.40
  19.2 2.1 fusion.36
  23.7 36.6 %all-reduce.3 = (f32[32]{0:T(128)S(1)}, f32[32]{0:T(128)S(1)}) all-reduce(f32[32]{0:T(128)S(1)} %exponential_dynamic-update-slice_fusion, f32[32]{0:T(128)S(1)} %exponential_dynamic-update-slice_fusion.1), channel_id=4, replica_groups=mesh['sp'=16,'tp'=2] {'sp'}, use_global_device_ids=true, to_apply=%add.1 | all-reduce | flops 64 | bytes 512
  61.8 1.6 broadcast_multiply_fusion
  63.4 1.7 copy.122
  65.1 1.7 copy.144
  70.5 19.9 %all-gather.15.cloned.1.call-done = f32[32,2,128,256]{3,2,1,0:T(8,128)} async-done(((f32[2,2,128,256]{3,2,1,0:T(8,128)}), f32[32,2,128,256]{3,2,1,0:T(8,128)}) %all-gather.15.cloned.1.call-update) | async-done | bytes 8388624 | tf_op jit(solution)/shard_map/all_gather | solution.py:12
  90.5 7.6 %rev.13 = f32[16,2,2,128,256]{4,3,2,1,0:T(8,128)} reverse(f32[16,2,2,128,256]{4,3,2,1,0:T(8,128)} %bitcast.160), dimensions={0} | reverse | bytes 16777216 | tf_op jit(solution)/shard_map/rev | solution.py:14
  98.1 67.5 %all-gather.17.cloned.1.call-done = f32[32,2,128,256]{3,2,1,0:T(8,128)} async-done(((f32[2,2,128,256]{3,2,1,0:T(8,128)}), f32[32,2,128,256]{3,2,1,0:T(8,128)}) %all-gather.17.cloned.1.call-update) | async-done | bytes 8388624 | tf_op jit(solution)/shard_map/all_gather | solution.py:12
  165.6 7.6 %rev.15 = f32[16,2,2,128,256]{4,3,2,1,0:T(8,128)} reverse(f32[16,2,2,128,256]{4,3,2,1,0:T(8,128)} %bitcast.161), dimensions={0} | reverse | bytes 16777216 | tf_op jit(solution)/shard_map/rev | solution.py:14
  173.1 42.3 %while.33 = (s32[]{:T(128)}, f32[2,2,128,256]{3,2,1,0:T(8,128)S(1)}, f32[2,2,128,256]{3,2,1,0:T(8,128)S(1)}, s32[]{:T(128)}, f32[16,1,2,1,1]{2,4,3,1,0:T(1,128)}...) while((s32[]{:T(128)}, ...), condition=%wide.region_3.4_spmd.clone, body=%wide.region_2.3_spmd.clone.sunk | while | flops 1048580 | bytes 3145917 | solution.py:24
  174.4 1.5 fusion.118
  199.5 1.8 fusion.118
  205.4 1.5 fusion.118
  208.2 1.5 fusion.118
  213.9 1.5 fusion.118
  218.0 22.7 %all-gather.11.cloned.1.call-done = f32[32,2,128,256]{3,2,1,0:T(8,128)} async-done(((f32[2,2,128,256]{3,2,1,0:T(8,128)}), f32[32,2,128,256]{3,2,1,0:T(8,128)}) %all-gather.11.cloned.1.call-update) | async-done | bytes 8388624 | tf_op jit(solution)/shard_map/all_gather | solution.py:12
  240.6 74.9 %all-gather.13.cloned.1.call-done = f32[32,2,128,256]{3,2,1,0:T(8,128)} async-done(((f32[2,2,128,256]{3,2,1,0:T(8,128)}), f32[32,2,128,256]{3,2,1,0:T(8,128)}) %all-gather.13.cloned.1.call-update) | async-done | bytes 8388624 | tf_op jit(solution)/shard_map/all_gather | solution.py:12
  315.6 23.2 %while.32 = (s32[]{:T(128)}, f32[2,2,128,256]{3,2,1,0:T(8,128)S(1)}, f32[2,2,128,256]{3,2,1,0:T(8,128)S(1)}, s32[]{:T(128)}, f32[16,1,2,1,1]{2,4,3,1,0:T(1,128)S...) while((s32[]{:T(128)}, ...), condition=%wide.region_1.2_spmd.clone, body=%wide.region_0.1_spmd.clone.sunk | while | flops 1048580 | bytes 3145917 | solution.py:24
  315.6 1.5 fusion.115
  317.2 1.5 fusion.115
  318.7 1.5 fusion.115
  341.3 1.8 fusion.38
  344.4 2.2 copy.136
  347.4 1.6 fusion.18
  351.7 31.6 %psum.7 = f32[2,2]{1,0:T(2,128)S(1)} all-reduce(f32[2,2]{1,0:T(2,128)S(1)} %pad_maximum_fusion), channel_id=1, replica_groups=mesh['sp'=16,'tp'=2] {'sp'}, use_global_device_ids=true, to_apply=%region_14.15 | all-reduce | flops 4 | bytes 32 | tf_op jit(solution)/shard_map/psum | solution.py:154
  383.3 1.7 fusion.28
  385.8 2.2 fusion.8
  392.8 46.6 %all-reduce.6.cloned.1.call-done = f32[1024,2,128]{2,1,0:T(2,128)} async-done(((f32[1024,2,128]{2,1,0:T(2,128)}), f32[1024,2,128]{2,1,0:T(2,128)}) %all-reduce.6.cloned.1.call-update) | async-done | bytes 1048592
  440.9 15.0 %reduce-scatter.2.cloned.1.call-done = bf16[1,128,1024]{2,1,0:T(8,128)(2,1)} async-done(((bf16[2,128,1024]{2,1,0:T(8,128)(2,1)}), bf16[1,128,1024]{2,1,0:T(8,128)(2,1)}) %reduce-scatter.2.cloned.1.call-update) | async-done | bytes 262160 | tf_op jit(solution)/shard_map/reduce_scatter | solution.py:34
  (169 shorter events, 80.6 us)
Async XLA Ops:
  7.2 2.8 copy-start
  7.2 62.4 %copy-start.2 = (bf16[2,128,2,256]{3,2,1,0:T(2,128)(2,1)S(1)}, bf16[2,128,2,256]{3,2,1,0:T(2,128)(2,1)}, u32[]{:S(2)}) copy-start(bf16[2,128,2,256]{3,2,1,0:T(2,128)(2,1)} %param.13) | copy-start | bytes 786436
  7.2 62.4 %copy-start.1 = (bf16[2,128,2,256]{3,2,1,0:T(2,128)(2,1)S(1)}, bf16[2,128,2,256]{3,2,1,0:T(2,128)(2,1)}, u32[]{:S(2)}) copy-start(bf16[2,128,2,256]{3,2,1,0:T(2,128)(2,1)} %param.14) | copy-start | bytes 786436
  7.2 83.3 %all-gather.15.cloned.1.call-start = ((), (), s32[]{:S(2)}) async-start(), calls=%async_computation.4 | async-start | bytes 8912896 | tf_op jit(solution)/shard_map/all_gather | solution.py:12
  9.9 11.6 %copy-start.12 = (f32[2]{0:T(128)}, f32[2]{0:T(128)S(1)}, u32[]{:S(2)}) copy-start(f32[2]{0:T(128)S(1)} %get-tuple-element.478) | copy-start | bytes 28
  9.9 11.6 %copy-start.13 = (f32[2]{0:T(128)}, f32[2]{0:T(128)S(1)}, u32[]{:S(2)}) copy-start(f32[2]{0:T(128)S(1)} %get-tuple-element.450) | copy-start | bytes 28
  10.9 10.5 %copy-start.8 = (f32[128,2]{0,1:T(2,128)}, f32[128,2]{0,1:T(2,128)S(1)}, u32[]{:S(2)}) copy-start(f32[128,2]{0,1:T(2,128)S(1)} %get-tuple-element.470) | copy-start | bytes 3076
  13.1 152.5 %all-gather.17.cloned.1.call-start = ((), (), s32[]{:S(2)}) async-start(), calls=%async_computation.5 | async-start | bytes 8912896 | tf_op jit(solution)/shard_map/all_gather | solution.py:12
  14.8 6.6 %copy-start.6 = (f32[128,2]{0,1:T(2,128)}, f32[128,2]{0,1:T(2,128)S(1)}, u32[]{:S(2)}) copy-start(f32[128,2]{0,1:T(2,128)S(1)} %get-tuple-element.467) | copy-start | bytes 3076
  17.0 223.6 %all-gather.11.cloned.1.call-start = ((), (), s32[]{:S(2)}) async-start(), calls=%async_computation.2 | async-start | bytes 8912896 | tf_op jit(solution)/shard_map/all_gather | solution.py:12
  19.2 296.4 %all-gather.13.cloned.1.call-start = ((), (), s32[]{:S(2)}) async-start(), calls=%async_computation.3 | async-start | bytes 8912896 | tf_op jit(solution)/shard_map/all_gather | solution.py:12
  21.4 418.0 %all-reduce.6.cloned.1.call-start = ((), (), s32[]{:S(2)}) async-start(), calls=%async_computation.6 | async-start | bytes 2097152
  173.1 42.3 %copy-start.9 = (f32[128,2]{0,1:T(2,128)S(1)}, f32[128,2]{0,1:T(2,128)}, u32[]{:S(2)}) copy-start(f32[128,2]{0,1:T(2,128)} %copy-done.8) | copy-start | bytes 3076
  315.6 25.4 %copy-start.3 = (f32[2,2,128,128]{3,2,1,0:T(8,128)S(1)}, f32[2,2,128,128]{3,2,1,0:T(8,128)}, u32[]{:S(2)}) copy-start(f32[2,2,128,128]{3,2,1,0:T(8,128)} %fusion.72) | copy-start | bytes 786436
  315.6 25.4 %copy-start.5 = (f32[2,128,128]{2,1,0:T(8,128)S(1)}, f32[2,128,128]{2,1,0:T(8,128)}, u32[]{:S(2)}) copy-start(f32[2,128,128]{2,1,0:T(8,128)} %get-tuple-element.459) | copy-start | bytes 393220
  338.7 8.0 %copy-start.7 = (f32[128,2]{0,1:T(2,128)S(1)}, f32[128,2]{0,1:T(2,128)}, u32[]{:S(2)}) copy-start(f32[128,2]{0,1:T(2,128)} %copy-done.6) | copy-start | bytes 3076
  338.8 8.6 %copy-start.4 = (f32[2,2,128,128]{2,3,1,0:T(8,128)S(1)}, f32[2,2,128,128]{2,3,1,0:T(8,128)}, u32[]{:S(2)}) copy-start(f32[2,2,128,128]{2,3,1,0:T(8,128)} %convolution_bitcast_fusion.16) | copy-start | bytes 786436
  339.9 48.1 %copy-start.10 = (f32[128,2]{0,1:T(2,128)S(1)}, f32[128,2]{0,1:T(2,128)}, u32[]{:S(2)}) copy-start(f32[128,2]{0,1:T(2,128)} %get-tuple-element.468) | copy-start | bytes 3076
  340.9 47.7 %copy-start.11 = (f32[128,2]{0,1:T(2,128)S(1)}, f32[128,2]{0,1:T(2,128)}, u32[]{:S(2)}) copy-start(f32[128,2]{0,1:T(2,128)} %get-tuple-element.461) | copy-start | bytes 3076
  346.7 109.2 %reduce-scatter.2.cloned.1.call-start = ((), (), s32[]{:S(2)}) async-start(), calls=%async_computation.1 | async-start | bytes 786432 | tf_op jit(solution)/shard_map/reduce_scatter | solution.py:34
Sparse Core Ops, SparseCore 0:
  13.2 77.2 all-gather.14
  92.6 72.8 all-gather.16
  167.7 72.8 all-gather.10
  242.6 72.8 all-gather.12
  346.8 92.5 all-reduce.5
  442.1 13.7 reduce-scatter.1
where the time goes:
time: 464 us; the launch traced here: 463 us
  waiting for transfers between devices  247 us (53%)
  blocking collectives  68.2 us (15%)
  other arithmetic  51.9 us (11%)
  local copies, waits for them, and re-layouts  49.5 us (11%)
  matrix products  29.3 us (6%)
  between operations  15.8 us (3%)
    all_gather x4, waiting for transfers between devices, prefix(): pieces = jax.tree.map(lambda part: lax.all_gather(part, axis), value)  185 us
    unnamed x7, waiting for transfers between devices  46.7 us
    select_n x30, other arithmetic, step(): jnp.where(position < mine, new, old)  44.9 us
    unnamed x1, blocking collectives  36.6 us
    psum x1, blocking collectives, shards(): rate_sums = lax.psum(local_sums, 'sp')  31.6 us
    rev x4, local copies, waits for them, and re-layouts, prefix(): pieces = jax.tree.map(lambda part: part[::-1], pieces)  16.4 us
    reduce_scatter x1, waiting for transfers between devices, summed_rows(): lax.psum_scatter(everything.astype(jnp.bfloat16), axis, scatter_dimension...  15 us
    mul x30, local copies, waits for them, and re-layouts, link_states(): later[0] * earlier[1] + later[1]  9.94 us
  transfers between devices with their start and end apart: 6, of which 6 were waited for; matrix products, arithmetic and copies ran while one was open for 20% of the time, Pallas kernels for 0%

commit v1 on v0

--- a/solution.py
+++ b/solution.py
@@ -151,7 +151,11 @@
     out_dot_behind = jnp.sum(positions * jnp.sum(out_behind * grad_wide, axis=3), axis=(0, 1))
     key_dot_behind = jnp.sum(positions * jnp.sum(keys * grad_k_behind, axis=3), axis=(0, 1))
     local_sums = jnp.stack([out_dot_ahead - key_dot_ahead, key_dot_behind - out_dot_behind])
-    rate_sums = lax.psum(local_sums, "sp")
+    rate_sums = local_sums
+    for hop in (1, 2, 4, 8):
+        rate_sums = rate_sums + lax.ppermute(
+            rate_sums, "sp", [(dev, dev ^ hop) for dev in range(16)]
+        )
     slopes = jnp.stack([jax.nn.sigmoid(-decay_ahead), jax.nn.sigmoid(-decay_behind)]) / all_tokens
     decay_grad = rate_sums * slopes
     key_grad_raw = ((grad_k_ahead + grad_k_behind) * key_scale).astype(jnp.bfloat16)

time: 464 us -> 495 us (1.067)
  waiting for transfers between devices: 247 us -> 303 us
  blocking collectives: 68.2 us -> 36.6 us
    psum x1 -> x0, blocking collectives: 31.6 us -> none  [shards(): rate_sums = lax.psum(local_sums, 'sp')]
    all_gather x4, waiting for transfers between devices: 185 us -> 212 us  [prefix(): pieces = jax.tree.map(lambda part: lax.all_gather(part, axis), value)]
    unnamed x7, waiting for transfers between devices: 46.7 us -> 67.5 us
    ppermute x0 -> x4, waiting for transfers between devices: none -> 8.89 us  [shards(): lax.ppermute(rate_sums, 'sp', [(dev, dev ^ hop) for dev in range(16)])]
  transfers between devices with their start and end apart: 6 -> 10, of which waited for: 6 -> 10; matrix products, arithmetic and copies ran while one was open for 20% -> 13% of each run, Pallas kernels for 0% -> 0%
where the time goes in v1:
time: 495 us; the launch traced here: 493 us
  waiting for transfers between devices  303 us (61%)
  other arithmetic  51.5 us (10%)
  local copies, waits for them, and re-layouts  50.7 us (10%)
  blocking collectives  36.6 us (7%)
  matrix products  30.4 us (6%)
  between operations  15.8 us (3%)
    all_gather x4, waiting for transfers between devices, prefix(): pieces = jax.tree.map(lambda part: lax.all_gather(part, axis), value)  212 us
    unnamed x7, waiting for transfers between devices  67.5 us
    select_n x30, other arithmetic, step(): jnp.where(position < mine, new, old)  44.5 us
    unnamed x1, blocking collectives  36.6 us
    rev x4, local copies, waits for them, and re-layouts, prefix(): pieces = jax.tree.map(lambda part: part[::-1], pieces)  16.4 us
    reduce_scatter x1, waiting for transfers between devices, summed_rows(): lax.psum_scatter(everything.astype(jnp.bfloat16), axis, scatter_dimension...  15 us
    mul x30, local copies, waits for them, and re-layouts, link_states(): later[0] * earlier[1] + later[1]  9.93 us
  transfers between devices with their start and end apart: 10, of which 10 were waited for; matrix products, arithmetic and copies ran while one was open for 13% of the time, Pallas kernels for 0%

profile of v1, /device:TPU:0, one launch (start us, length us, event | category | flops | bytes accessed | tf_op | source)
XLA Modules:
  0.0 493.5 jit_solution(2948486079307827320)
XLA Ops:
  10.9 2.2 fusion.41
  13.8 2.1 fusion.40
  17.1 2.1 fusion.36
  19.3 2.1 fusion.37
  23.8 36.6 %all-reduce.3 = (f32[32]{0:T(128)S(1)}, f32[32]{0:T(128)S(1)}) all-reduce(f32[32]{0:T(128)S(1)} %exponential_dynamic-update-slice_fusion, f32[32]{0:T(128)S(1)} %exponential_dynamic-update-slice_fusion.1), channel_id=4, replica_groups=mesh['sp'=16,'tp'=2] {'sp'}, use_global_device_ids=true, to_apply=%add.1 | all-reduce | flops 64 | bytes 512
  61.9 1.6 broadcast_multiply_fusion
  63.5 1.6 copy.122
  65.1 1.6 copy.144
  70.5 20.0 %all-gather.15.cloned.1.call-done = f32[32,2,128,256]{3,2,1,0:T(8,128)} async-done(((f32[2,2,128,256]{3,2,1,0:T(8,128)}), f32[32,2,128,256]{3,2,1,0:T(8,128)}) %all-gather.15.cloned.1.call-update) | async-done | bytes 8388624 | tf_op jit(solution)/shard_map/all_gather | solution.py:12
  90.5 7.6 %rev.13 = f32[16,2,2,128,256]{4,3,2,1,0:T(8,128)} reverse(f32[16,2,2,128,256]{4,3,2,1,0:T(8,128)} %bitcast.161), dimensions={0} | reverse | bytes 16777216 | tf_op jit(solution)/shard_map/rev | solution.py:14
  98.1 67.5 %all-gather.11.cloned.1.call-done = f32[32,2,128,256]{3,2,1,0:T(8,128)} async-done(((f32[2,2,128,256]{3,2,1,0:T(8,128)}), f32[32,2,128,256]{3,2,1,0:T(8,128)}) %all-gather.11.cloned.1.call-update) | async-done | bytes 8388624 | tf_op jit(solution)/shard_map/all_gather | solution.py:12
  165.6 75.1 %all-gather.13.cloned.1.call-done = f32[32,2,128,256]{3,2,1,0:T(8,128)} async-done(((f32[2,2,128,256]{3,2,1,0:T(8,128)}), f32[32,2,128,256]{3,2,1,0:T(8,128)}) %all-gather.13.cloned.1.call-update) | async-done | bytes 8388624 | tf_op jit(solution)/shard_map/all_gather | solution.py:12
  240.7 23.3 %while.32 = (s32[]{:T(128)}, f32[2,2,128,256]{3,2,1,0:T(8,128)S(1)}, f32[2,2,128,256]{3,2,1,0:T(8,128)S(1)}, s32[]{:T(128)}, f32[16,1,2,1,1]{2,4,3,1,0:T(1,128)S...) while((s32[]{:T(128)}, ...), condition=%wide.region_1.2_spmd.clone, body=%wide.region_0.1_spmd.clone.sunk | while | flops 1048580 | bytes 3145917 | solution.py:24
  248.4 1.6 fusion.117
  250.0 1.5 fusion.117
  259.3 1.5 fusion.117
  260.9 1.5 fusion.117
  262.4 1.5 fusion.117
  266.5 49.1 %all-gather.17.cloned.1.call-done = f32[32,2,128,256]{3,2,1,0:T(8,128)} async-done(((f32[2,2,128,256]{3,2,1,0:T(8,128)}), f32[32,2,128,256]{3,2,1,0:T(8,128)}) %all-gather.17.cloned.1.call-update) | async-done | bytes 8388624 | tf_op jit(solution)/shard_map/all_gather | solution.py:12
  315.6 7.6 %rev.15 = f32[16,2,2,128,256]{4,3,2,1,0:T(8,128)} reverse(f32[16,2,2,128,256]{4,3,2,1,0:T(8,128)} %bitcast.160), dimensions={0} | reverse | bytes 16777216 | tf_op jit(solution)/shard_map/rev | solution.py:14
  323.2 42.0 %while.33 = (s32[]{:T(128)}, f32[2,2,128,256]{3,2,1,0:T(8,128)S(1)}, f32[2,2,128,256]{3,2,1,0:T(8,128)S(1)}, s32[]{:T(128)}, f32[16,1,2,1,1]{2,4,3,1,0:T(1,128)}...) while((s32[]{:T(128)}, ...), condition=%wide.region_3.4_spmd.clone, body=%wide.region_2.3_spmd.clone.sunk | while | flops 1048580 | bytes 3145917 | solution.py:24
  369.7 2.2 fusion.8
  375.3 2.2 copy.136
  377.9 2.2 fusion.17
  380.1 1.7 fusion.28
  382.6 1.9 copy.151
  390.4 3.0 collective-permute-done.1
  394.7 2.3 collective-permute-done.2
  397.1 1.8 collective-permute-start.3
  398.9 2.6 collective-permute-done.3
  402.8 67.4 %all-reduce.6.cloned.1.call-done = f32[1024,2,128]{2,1,0:T(2,128)} async-done(((f32[1024,2,128]{2,1,0:T(2,128)}), f32[1024,2,128]{2,1,0:T(2,128)}) %all-reduce.6.cloned.1.call-update) | async-done | bytes 1048592
  471.7 15.0 %reduce-scatter.2.cloned.1.call-done = bf16[1,128,1024]{2,1,0:T(8,128)(2,1)} async-done(((bf16[2,128,1024]{2,1,0:T(8,128)(2,1)}), bf16[1,128,1024]{2,1,0:T(8,128)(2,1)}) %reduce-scatter.2.cloned.1.call-update) | async-done | bytes 262160 | tf_op jit(solution)/shard_map/reduce_scatter | solution.py:34
  (183 shorter events, 89.8 us)
Async XLA Ops:
  7.2 2.8 copy-start
  7.2 62.4 %copy-start.2 = (bf16[2,128,2,256]{3,2,1,0:T(2,128)(2,1)S(1)}, bf16[2,128,2,256]{3,2,1,0:T(2,128)(2,1)}, u32[]{:S(2)}) copy-start(bf16[2,128,2,256]{3,2,1,0:T(2,128)(2,1)} %param.13) | copy-start | bytes 786436
  7.2 62.4 %copy-start.1 = (bf16[2,128,2,256]{3,2,1,0:T(2,128)(2,1)S(1)}, bf16[2,128,2,256]{3,2,1,0:T(2,128)(2,1)}, u32[]{:S(2)}) copy-start(bf16[2,128,2,256]{3,2,1,0:T(2,128)(2,1)} %param.14) | copy-start | bytes 786436
  7.2 83.3 %all-gather.15.cloned.1.call-start = ((), (), s32[]{:S(2)}) async-start(), calls=%async_computation.4 | async-start | bytes 8912896 | tf_op jit(solution)/shard_map/all_gather | solution.py:12
  9.9 11.6 %copy-start.14 = (f32[2]{0:T(128)}, f32[2]{0:T(128)S(1)}, u32[]{:S(2)}) copy-start(f32[2]{0:T(128)S(1)} %get-tuple-element.478) | copy-start | bytes 28
  9.9 11.6 %copy-start.15 = (f32[2]{0:T(128)}, f32[2]{0:T(128)S(1)}, u32[]{:S(2)}) copy-start(f32[2]{0:T(128)S(1)} %get-tuple-element.450) | copy-start | bytes 28
  10.9 10.5 %copy-start.8 = (f32[128,2]{0,1:T(2,128)}, f32[128,2]{0,1:T(2,128)S(1)}, u32[]{:S(2)}) copy-start(f32[128,2]{0,1:T(2,128)S(1)} %get-tuple-element.470) | copy-start | bytes 3076
  13.1 152.5 %all-gather.11.cloned.1.call-start = ((), (), s32[]{:S(2)}) async-start(), calls=%async_computation.2 | async-start | bytes 8912896 | tf_op jit(solution)/shard_map/all_gather | solution.py:12
  13.8 7.6 %copy-start.10 = (f32[128,2]{0,1:T(2,128)}, f32[128,2]{0,1:T(2,128)S(1)}, u32[]{:S(2)}) copy-start(f32[128,2]{0,1:T(2,128)S(1)} %get-tuple-element.467) | copy-start | bytes 3076
  16.0 224.7 %all-gather.13.cloned.1.call-start = ((), (), s32[]{:S(2)}) async-start(), calls=%async_computation.3 | async-start | bytes 8912896 | tf_op jit(solution)/shard_map/all_gather | solution.py:12
  19.2 296.4 %all-gather.17.cloned.1.call-start = ((), (), s32[]{:S(2)}) async-start(), calls=%async_computation.5 | async-start | bytes 8912896 | tf_op jit(solution)/shard_map/all_gather | solution.py:12
  21.4 448.8 %all-reduce.6.cloned.1.call-start = ((), (), s32[]{:S(2)}) async-start(), calls=%async_computation.6 | async-start | bytes 2097152
  98.1 165.8 %copy-start.13 = (f32[128,2]{0,1:T(2,128)S(1)}, f32[128,2]{0,1:T(2,128)}, u32[]{:S(2)}) copy-start(f32[128,2]{0,1:T(2,128)} %get-tuple-element.468) | copy-start | bytes 3076
  323.2 42.1 %copy-start.12 = (f32[128,2]{0,1:T(2,128)S(1)}, f32[128,2]{0,1:T(2,128)}, u32[]{:S(2)}) copy-start(f32[128,2]{0,1:T(2,128)} %get-tuple-element.461) | copy-start | bytes 3076
  323.2 43.9 %copy-start.3 = (f32[2,2,128,128]{3,2,1,0:T(8,128)S(1)}, f32[2,2,128,128]{3,2,1,0:T(8,128)}, u32[]{:S(2)}) copy-start(f32[2,2,128,128]{3,2,1,0:T(8,128)} %fusion.72) | copy-start | bytes 786436
  323.2 43.9 %copy-start.7 = (f32[2,128,128]{2,1,0:T(8,128)S(1)}, f32[2,128,128]{2,1,0:T(8,128)}, u32[]{:S(2)}) copy-start(f32[2,128,128]{2,1,0:T(8,128)} %get-tuple-element.459) | copy-start | bytes 393220
  323.2 50.0 %copy-start.9 = (f32[128,2]{0,1:T(2,128)S(1)}, f32[128,2]{0,1:T(2,128)}, u32[]{:S(2)}) copy-start(f32[128,2]{0,1:T(2,128)} %copy-done.8) | copy-start | bytes 3076
  323.2 51.0 %copy-start.11 = (f32[128,2]{0,1:T(2,128)S(1)}, f32[128,2]{0,1:T(2,128)}, u32[]{:S(2)}) copy-start(f32[128,2]{0,1:T(2,128)} %copy-done.10) | copy-start | bytes 3076
  365.3 12.6 %copy-start.4 = (f32[2,2,128,128]{2,3,1,0:T(8,128)S(1)}, f32[2,2,128,128]{2,3,1,0:T(8,128)}, u32[]{:S(2)}) copy-start(f32[2,2,128,128]{2,3,1,0:T(8,128)} %convolution_bitcast_fusion.16) | copy-start | bytes 786436
  367.1 10.8 %copy-start.5 = (f32[2,128,2,256]{3,1,2,0:T(8,128)S(1)}, f32[2,128,2,256]{3,1,2,0:T(8,128)}, u32[]{:S(2)}) copy-start(f32[2,128,2,256]{3,1,2,0:T(8,128)} %fusion.16) | copy-start | bytes 1572868
  373.2 14.1 %copy-start.6 = (f32[2,128,128]{1,2,0:T(8,128)S(1)}, f32[2,128,128]{1,2,0:T(8,128)}, u32[]{:S(2)}) copy-start(f32[2,128,128]{1,2,0:T(8,128)} %copy.137) | copy-start | bytes 393220
  377.6 109.0 %reduce-scatter.2.cloned.1.call-start = ((), (), s32[]{:S(2)}) async-start(), calls=%async_computation.1 | async-start | bytes 786432 | tf_op jit(solution)/shard_map/reduce_scatter | solution.py:34
  388.6 1.2 collective-permute-start
  389.8 3.6 collective-permute-start.1
  393.4 3.6 collective-permute-start.2
  397.1 4.5 collective-permute-start.3
Sparse Core Ops, SparseCore 0:
  13.2 77.2 all-gather.14
  92.7 72.8 all-gather.10
  167.7 72.8 all-gather.12
  242.7 72.8 all-gather.16
  377.7 92.3 all-reduce.5
  472.9 13.7 reduce-scatter.1
